TPU v7x, 256 devices: a whole 4x4x8 slice. The times are simulated.
256 devices in a mesh: fs: 16 (over y, x), tp: 16 (over z, core).
Axes of the slice: x: 4, y: 4, z: 8, core: 2. Of those that a mesh axis runs over, the one named last changes fastest.
Arguments:
- tokens: bfloat16 [32768, 2048], P(('fs', 'tp')), may hold values from -6 to 6
- norm_gain: float32 [2048], replicated, may hold values from 0.1 to 1.9
- gate_weight: bfloat16 [2048, 5632], P('fs', 'tp'), may hold values from -0.125 to 0.125
- up_weight: bfloat16 [2048, 5632], P('fs', 'tp'), may hold values from -0.125 to 0.125
- down_weight: bfloat16 [5632, 2048], P('tp', 'fs'), may hold values from -0.078125 to 0.078125
Outputs:
- mixed: bfloat16 [32768, 2048], P(('fs', 'tp'))
All inputs are finite; a program needn't handle non-finite values.
Results may differ from a plain program's by a relative error of at most 0.0065.
Values may be sent and summed in bfloat16 or wider, within the bound.
A program may use at most 128 MiB of HBM per device.

v0:
```python
import jax
import jax.numpy as jnp
from jax import lax
from jax.sharding import PartitionSpec as P

eps_floor = 0.05


def sent_together(arrays, axis, dim, along):
    both = jnp.concatenate(arrays, axis=along)
    out, at, outs = (lax.all_gather(both, axis, axis=dim, tiled=True), 0, [])
    for a in arrays:
        outs.append(lax.slice_in_dim(out, at, at + a.shape[along], axis=along))
        at += a.shape[along]
    return tuple(outs)


def joined_along(blocks, dim):
    blocks = jnp.moveaxis(blocks, 0, dim)
    lengths = blocks.shape
    return blocks.reshape(*lengths[:dim], lengths[dim] * lengths[dim + 1], *lengths[dim + 2 :])


def from_everyone(x, axis):
    length = lax.axis_size(axis)
    return lax.all_to_all(jnp.broadcast_to(x[None], (length, *x.shape)), axis, 0, 0, tiled=True)


def collect(x, axis, dim):
    return joined_along(from_everyone(x, axis), dim)


def local(tokens, norm_gain, gate_weight, up_weight, down_weight):
    values = tokens.astype(jnp.float32)
    factor = lax.rsqrt(jnp.mean(values * values, axis=-1, keepdims=True) + eps_floor)
    normed = (values * factor * norm_gain).astype(jnp.bfloat16)
    gate_full, upper_full = sent_together((gate_weight, up_weight), "fs", 0, 1)
    piece = lax.all_gather(normed, "tp", axis=0, tiled=True)
    gate = jnp.dot(piece, gate_full, preferred_element_type=jnp.float32)
    upper = jnp.dot(piece, upper_full, preferred_element_type=jnp.float32)
    hidden = (jax.nn.silu(gate) * upper).astype(jnp.bfloat16)
    down_local = collect(down_weight, "fs", 1)
    mixed = lax.psum_scatter(
        jnp.dot(hidden, down_local, preferred_element_type=jnp.float32),
        "tp",
        scatter_dimension=0,
        tiled=True,
    )
    return mixed.astype(jnp.bfloat16)


def solution(mesh):
    return jax.shard_map(
        local,
        mesh=mesh,
        in_specs=(P(("fs", "tp"), None), P(), P("fs", "tp"), P("fs", "tp"), P("tp", "fs")),
        out_specs=P(("fs", "tp"), None),
        check_vma=False,
    )
```

profile of v0, /device:TPU:32, one launch (start us, length us, event | category | flops | bytes accessed | tf_op | source)
XLA Modules:
  0.0 258.2 jit_solution(3198704871677870176)
XLA Ops:
  6.5 0.0 all-gather.5.cloned.1.call-start
  6.5 1.6 pad_maximum_fusion
  8.1 0.0 all-gather.5.cloned.1.call-update
  8.2 0.0 all-gather.3.cloned.1.call-start
  8.2 1.2 fusion.7
  9.5 2.0 fusion.9
  11.5 0.0 all-gather.3.cloned.1.call-update
  11.5 2.2 broadcast_in_dim.2
  13.7 7.0 %all-to-all-start = ((bf16[16,352,128]{2,1,0:T(8,128)(2,1)}), bf16[16,352,128]{2,1,0:T(8,128)(2,1)S(1)}, u32[]{:S(2)}, u32[]{:S(2)}) async-start(bf16[16,352,128]{2,1,0:T(8,128)(2,1)} %broadcast_in_dim.2), calls=%async_computation | async-start | bytes 2883584 | tf_op jit(solution)/shard_map/all_to_all | solution.py:26
  20.8 0.0 reduce-scatter.2.cloned.1.call-start
  20.8 56.7 %all-gather.5.cloned.1.call-done = bf16[2048,704]{0,1:T(8,128)(2,1)} async-done(((bf16[128,704]{0,1:T(8,128)(2,1)}), bf16[2048,704]{0,1:T(8,128)(2,1)}) %all-gather.5.cloned.1.call-update) | async-done | bytes 2883600 | tf_op jit(solution)/shard_map/all_gather | solution.py:11
  77.5 55.3 %all-gather.3.cloned.1.call-done = bf16[2048,2048]{1,0:T(8,128)(2,1)} async-done(((bf16[128,2048]{1,0:T(8,128)(2,1)}), bf16[2048,2048]{1,0:T(8,128)(2,1)}) %all-gather.3.cloned.1.call-update) | async-done | bytes 8388624 | tf_op jit(solution)/shard_map/all_gather | solution.py:38
  132.8 0.0 copy-start
  132.8 0.0 copy-start.1
  132.8 6.4 %fusion.5 = f32[2048,352]{0,1:T(8,128)S(1)} fusion(bf16[2048,2048]{1,0:T(8,128)(2,1)} %all-gather.3.cloned.1.call-done, bf16[2048,704]{0,1:T(8,128)(2,1)} %all-gather.5.cloned.1.call-done), kind=kOutput, calls=%fused_computation.6 | convolution fusion | flops 2952790016 | bytes 12713984 | tf_op jit(solution)/shard_map/dot_general | solution.py:39
  139.3 0.0 copy-done
  139.3 0.6 copy-done.1
  139.9 3.5 %fusion = bf16[2048,352]{0,1:T(8,128)(2,1)S(1)} fusion(bf16[2048,2048]{1,0:T(8,128)(2,1)S(1)} %copy-done, f32[2048,352]{0,1:T(8,128)S(1)} %fusion.5, bf16[2048,704]{0,1:T(8,128)(2,1)S(1)} %copy-done.1), kind=kOutput, calls=%fused_computation.1 | convolution fusion | flops 2957115392 | bytes 14155776 | tf_op jit(solution)/shard_map/dot_general | solution.py:40
  143.4 0.0 all-to-all-done
  143.4 8.1 %fusion.1 = f32[2048,2048]{1,0:T(8,128)} fusion(bf16[2048,352]{0,1:T(8,128)(2,1)S(1)} %fusion, bf16[16,352,128]{2,1,0:T(8,128)(2,1)S(1)} %all-to-all-done), kind=kOutput, calls=%fused_computation.2 | convolution fusion | flops 2952790016 | bytes 19660800 | tf_op jit(solution)/shard_map/dot_general | solution.py:44
  151.6 0.0 reduce-scatter.2.cloned.1.call-update
  151.6 98.1 %reduce-scatter.2.cloned.1.call-done = f32[128,2048]{1,0:T(8,128)} async-done(((f32[2048,2048]{1,0:T(8,128)}), f32[128,2048]{1,0:T(8,128)}) %reduce-scatter.2.cloned.1.call-update) | async-done | bytes 1048592 | tf_op jit(solution)/shard_map/reduce_scatter | solution.py:43
  249.6 2.1 convert_element_type.15
  (1 shorter events, 0.0 us)
Async XLA Ops:
  6.5 71.0 %all-gather.5.cloned.1.call-start = ((), (), s32[]{:S(2)}) async-start(), calls=%async_computation.3 | async-start | bytes 3063808 | tf_op jit(solution)/shard_map/all_gather | solution.py:11
  8.2 124.7 %all-gather.3.cloned.1.call-start = ((), (), s32[]{:S(2)}) async-start(), calls=%async_computation.2 | async-start | bytes 8912896 | tf_op jit(solution)/shard_map/all_gather | solution.py:38
  13.7 129.7 %all-to-all-start = ((bf16[16,352,128]{2,1,0:T(8,128)(2,1)}), bf16[16,352,128]{2,1,0:T(8,128)(2,1)S(1)}, u32[]{:S(2)}, u32[]{:S(2)}) async-start(bf16[16,352,128]{2,1,0:T(8,128)(2,1)} %broadcast_in_dim.2), calls=%async_computation | async-start | bytes 2883584 | tf_op jit(solution)/shard_map/all_to_all | solution.py:26
  20.8 228.9 %reduce-scatter.2.cloned.1.call-start = ((), (), s32[]{:S(2)}) async-start(), calls=%async_computation.4 | async-start | bytes 17825792 | tf_op jit(solution)/shard_map/reduce_scatter | solution.py:43
  132.8 6.4 %copy-start = (bf16[2048,2048]{1,0:T(8,128)(2,1)S(1)}, bf16[2048,2048]{1,0:T(8,128)(2,1)}, u32[]{:S(2)}) copy-start(bf16[2048,2048]{1,0:T(8,128)(2,1)} %all-gather.3.cloned.1.call-done) | copy-start | bytes 25165828
  132.8 7.1 %copy-start.1 = (bf16[2048,704]{0,1:T(8,128)(2,1)S(1)}, bf16[2048,704]{0,1:T(8,128)(2,1)}, u32[]{:S(2)}) copy-start(bf16[2048,704]{0,1:T(8,128)(2,1)} %all-gather.5.cloned.1.call-done) | copy-start | bytes 8650756
Sparse Core Ops, SparseCore 0:
  9.7 67.7 all-gather.4
  79.4 53.4 all-gather.2
  151.7 97.8 reduce-scatter.1
where the time goes:
time: 262 us; the launch traced here: 258 us
  waiting for transfers between devices  210 us (80%)
  matrix products  18 us (7%)
  between operations  13.1 us (5%)
  starting transfers between devices  7.12 us (3%)
  other arithmetic  6.96 us (3%)
  local copies, waits for them, and re-layouts  2.83 us (1%)
    reduce_scatter x1, waiting for transfers between devices, local(): lax.psum_scatter(jnp.dot(hidden, down_local, preferred_element_type=jnp.f...  98.1 us
    all_gather x1, waiting for transfers between devices, sent_together(): out, at, outs = (lax.all_gather(both, axis, axis=dim, tiled=True), 0, [])  56.7 us
    all_gather x1, waiting for transfers between devices, local(): piece = lax.all_gather(normed, 'tp', axis=0, tiled=True)  55.3 us
    dot_general x1, matrix products, local(): jnp.dot(hidden, down_local, preferred_element_type=jnp.float32)  8.11 us
    all_to_all x1, starting transfers between devices, from_everyone(): lax.all_to_all(jnp.broadcast_to(x[None], (length, *x.shape)), axis, 0, 0,...  7.03 us
    dot_general x1, matrix products, local(): gate = jnp.dot(piece, gate_full, preferred_element_type=jnp.float32)  6.42 us
  transfers between devices with their start and end apart: 4, of which 3 were waited for; matrix products, arithmetic and copies ran while one was open for 6% of the time, Pallas kernels for 0%

commit v1 on v0

v1 whole, which is shorter than its diff:
```python
import jax
import jax.numpy as jnp
from jax import lax
from jax.experimental import pallas as pl
from jax.experimental.pallas import tpu as pltpu
from jax.sharding import PartitionSpec as P

MESH = pl.DeviceIdType.MESH
BF, F32 = jnp.bfloat16, jnp.float32
eps_floor = 0.05

D, T, HU, HP = 2048, 128, 352, 384
GU_A, GU_B, D_A, D_B = 0, 1, 2, 3
PAIRS = (
    ((0, 0), (0, 1)),
    ((0, -1), (1, 0)),
    ((-1, 0), (2, 0)),
    ((1, 1), (1, -1)),
    ((-1, 1), (-1, -1)),
    ((0, 2), (1, 2)),
    ((-1, 2), (2, 1)),
    ((2, -1), (2, 2)),
)


def kernel(tok, gain, gate, up, down, out, wg, wd, x4, nrm, acc, hid, pb, rb, own, stage,
           in_sem, ssem, rsem, dsend, drecv_g, drecv_d, zsend, zrecv, tsend, trecv, psend, precv):
    fs, tp = lax.axis_index("fs"), lax.axis_index("tp")
    y, x, z, c = fs // 4, fs % 4, tp // 2, tp % 2
    d = 1 - 2 * c
    par = (x + y) % 2
    pars = (par, 1 - par, 1 - par, par)
    sibling = (fs, z * 2 + 1 - c)

    def zdev(k):
        return (fs, ((z + k + 8) % 8) * 2 + c)

    def fpos(t, i, j):
        p = pars[t]
        yy = (y + i * p + j * (1 - p) + 8) % 4
        xx = (x + i * (1 - p) + j * p + 8) % 4
        return yy * 4 + xx

    def piece(t, core, f):
        if t < 2:
            return wg.at[core, t, f]
        return wd.at[f, core * 2 + (t - 2), pl.ds(0, HU), :]

    def rcopy(src, dst, s, r, dev):
        return pltpu.make_async_remote_copy(
            src_ref=src, dst_ref=dst, send_sem=s, recv_sem=r, device_id=dev, device_id_type=MESH
        )

    def send(t, src, to):
        f = fpos(t, *src)
        ref = piece(t, c, f)
        rcopy(ref, ref, ssem.at[t], rsem.at[t, f], (fpos(t, *to), tp)).start()

    def across(t, src):
        f = fpos(t, *src)
        ref = piece(t, c, f)
        r = drecv_g.at[t] if t < 2 else drecv_d.at[t - 2, f]
        rcopy(ref, ref, dsend.at[t], r, sibling).start()

    def got(t, src):
        f = fpos(t, *src)
        ref = piece(t, c, f)
        rcopy(ref, ref, ssem.at[t], rsem.at[t, f], sibling).wait_recv()

    def s1(t):
        for to in ((1, 0), (-1, 0), (0, 1), (0, -1)):
            send(t, (0, 0), to)
        across(t, (0, 0))

    def s2(t):
        got(t, (0, -d))
        send(t, (0, -d), (0, d))
        send(t, (0, -d), (1, 0))
        send(t, (0, -d), (-1, 0))
        got(t, (0, d))
        send(t, (0, d), (1, 0))
        send(t, (0, d), (-1, 0))
        got(t, (-d, 0))
        send(t, (-d, 0), (d, 0))
        got(t, (d, 0))
        for src in ((0, -d), (0, d), (-d, 0), (d, 0)):
            across(t, src)

    def s3(t):
        got(t, (2, 0))
        send(t, (2, 0), (0, 1))
        send(t, (2, 0), (0, -1))
        for i in (1, -1):
            got(t, (i, -d))
            send(t, (i, -d), (0, d))
        for src in ((1, d), (-1, d), (0, 2)):
            got(t, src)
        for src in ((2, 0), (1, -d), (-1, -d), (1, d), (-1, d), (0, 2)):
            across(t, src)

    def s4(t):
        got(t, (-d, 2))
        send(t, (-d, 2), (d, 0))
        for src in ((d, 2), (2, 1), (2, -1)):
            got(t, src)
        for src in ((-d, 2), (d, 2), (2, 1), (2, -1)):
            across(t, src)

    def s5(t):
        got(t, (2, 2))
        across(t, (2, 2))

    def normalize(slot):
        def rows(i, _):
            at = pl.multiple_of(i * 16, 16)
            v = x4[slot, pl.ds(at, 16), :].astype(F32)
            factor = lax.rsqrt(jnp.sum(v * v, axis=-1, keepdims=True) * (1.0 / D) + eps_floor)
            nrm[pl.ds(pl.multiple_of(slot * T + at, 16), 16), :] = (v * factor * gain[...]).astype(BF)
            return 0

        lax.fori_loop(0, T // 16, rows, 0)

    def gate_up(core, ab):
        def columns(n, _):
            at = pl.multiple_of(n * 256, 256)
            w = wg[core, ab, :, :, pl.ds(at, 256)].reshape(D, 256)
            acc[:, pl.ds(at, 256)] = jnp.dot(nrm[...], w, preferred_element_type=F32)
            return 0

        lax.fori_loop(0, 3, columns, 0)
        lanes = pl.ds(pl.multiple_of((core * 2 + ab) * HP, 128), HP)

        def rows(i, _):
            at = pl.ds(pl.multiple_of(i * 32, 32), 32)
            g = acc[at, 0:HP]
            u = acc[at, HP : 2 * HP]
            hid[at, lanes] = (g / (1.0 + jnp.exp(-g)) * u).astype(BF)
            return 0

        lax.fori_loop(0, 16, rows, 0)

    def pair_fs(p):
        return [fpos(D_A, *o) for o in PAIRS[p]]

    def down_pair(p):
        fa, fb = pair_fs(p)
        for t in (D_A, D_B):
            for f in (fa, fb):
                ref = piece(t, 1 - c, f)
                rcopy(ref, ref, dsend.at[t], drecv_d.at[t - 2, f], sibling).wait_recv()
        w = jnp.concatenate([wd[fa].reshape(4 * HP, 128), wd[fb].reshape(4 * HP, 128)], axis=1)
        part = jnp.dot(hid[...], w, preferred_element_type=F32)
        for s in (1, 2, 3):
            for h in (0, 1):
                pb[p, s - 1, h] = part[s * T : (s + 1) * T, h * 128 : (h + 1) * 128].astype(BF)
        own[p] = part[0:T]
        for s, k in ((3, -2 * d), (1, -d), (2, d)):
            rcopy(pb.at[p, s - 1], rb.at[s - 1, p], psend, precv.at[s - 1, p], zdev(k)).start()

    def finish(p):
        for s in (0, 1, 2):
            rcopy(rb.at[s, p], rb.at[s, p], psend, precv.at[s, p], sibling).wait_recv()
        for h, f in enumerate(pair_fs(p)):
            v = own[p, :, h * 128 : (h + 1) * 128]
            for s in (0, 1, 2):
                v = v + rb[s, p, h].astype(F32)
            out[:, pl.ds(pl.multiple_of(f * 128, 128), 128)] = v.astype(BF)

    gd = pltpu.make_async_copy(gate, stage.at[0], in_sem.at[0])
    ud = pltpu.make_async_copy(up, stage.at[1], in_sem.at[1])
    dd = pltpu.make_async_copy(down, piece(D_A, c, fs), in_sem.at[2])
    td = pltpu.make_async_copy(tok, x4.at[0], in_sem.at[3])
    for cp in (gd, ud, dd, td):
        cp.start()
    barrier = pltpu.get_barrier_semaphore()
    partners = [sibling] + [(fpos(0, *o), tp) for o in ((1, 0), (-1, 0), (0, 1), (0, -1))]
    partners += [zdev(k) for k in (1, -1, 2, -2, 4)]
    for dev in partners:
        pl.semaphore_signal(barrier, inc=1, device_id=dev, device_id_type=MESH)
    for f in range(16):
        for b in range(4):
            wd[f, b, HU:HP, :] = jnp.zeros((HP - HU, 128), BF)
    gd.wait()
    ud.wait()
    pad = jnp.zeros((T, HP - HU), BF)
    wg[c, 0, fs, :, 0:HP] = jnp.concatenate([stage[0], pad], axis=1)
    wg[c, 0, fs, :, HP : 2 * HP] = jnp.concatenate([stage[1], pad], axis=1)
    dd.wait()
    td.wait()
    pl.semaphore_wait(barrier, len(partners))

    s1(GU_A)
    gz = rcopy(piece(GU_A, c, fs), piece(GU_B, c, fs), zsend.at[0], zrecv.at[0], zdev(4))
    gz.start()
    t2 = rcopy(x4.at[0], x4.at[2], tsend, trecv.at[2], zdev(-d))
    t1 = rcopy(x4.at[0], x4.at[1], tsend, trecv.at[1], zdev(d))
    t3 = rcopy(x4.at[1], x4.at[3], tsend, trecv.at[3], zdev(d))
    dz = rcopy(piece(D_A, c, fs), piece(D_B, c, fs), zsend.at[1], zrecv.at[1], zdev(4))
    t2.start()
    t1.start()
    s1(D_A)
    s2(GU_A)
    gz.wait_recv()
    s1(GU_B)
    s2(D_A)
    t1.wait_recv()
    t3.start()
    dz.start()
    s3(GU_A)
    s2(GU_B)
    s4(GU_A)
    s3(GU_B)
    s5(GU_A)
    normalize(0)
    normalize(1)
    s4(GU_B)
    dz.wait_recv()
    s1(D_B)
    s3(D_A)
    t2.wait_recv()
    normalize(2)
    t3.wait_recv()
    normalize(3)
    rcopy(wg.at[1 - c, 0], wg.at[1 - c, 0], dsend.at[0], drecv_g.at[0], sibling).wait_recv()
    gate_up(c, 0)
    s2(D_B)
    s4(D_A)
    gate_up(1 - c, 0)
    s5(GU_B)
    gate_up(c, 1)
    s3(D_B)
    s5(D_A)
    rcopy(wg.at[1 - c, 1], wg.at[1 - c, 1], dsend.at[1], drecv_g.at[1], sibling).wait_recv()
    gate_up(1 - c, 1)
    s4(D_B)
    down_pair(0)
    down_pair(1)
    s5(D_B)
    for p in range(2, 8):
        down_pair(p)
        finish(p - 2)
    finish(6)
    finish(7)

    for t in (GU_A, GU_B):
        few = wg.at[c, t, pl.ds(0, 15)]
        rcopy(few, few, ssem.at[t], rsem.at[t, 0], sibling).wait_send()
        rcopy(wg.at[c, t], wg.at[c, t], dsend.at[t], drecv_g.at[t], sibling).wait_send()
    for t in (D_A, D_B):
        few = wd.at[pl.ds(0, 15), 0, pl.ds(0, HU), :]
        rcopy(few, few, ssem.at[t], rsem.at[t, 0], sibling).wait_send()
        all16 = wd.at[:, 0, pl.ds(0, HU), :]
        rcopy(all16, all16, dsend.at[t], drecv_d.at[t - 2, 0], sibling).wait_send()
    gz.wait_send()
    dz.wait_send()
    three = x4.at[pl.ds(0, 3)]
    rcopy(three, three, tsend, trecv.at[1], sibling).wait_send()
    rcopy(pb, pb, psend, precv.at[0, 0], sibling).wait_send()


def local(tokens, norm_gain, gate_weight, up_weight, down_weight):
    hbm = pl.BlockSpec(memory_space=pl.ANY)
    vmem = pl.BlockSpec(memory_space=pltpu.VMEM)
    dma = pltpu.SemaphoreType.DMA
    return pl.pallas_call(
        kernel,
        out_shape=jax.ShapeDtypeStruct((T, D), BF),
        in_specs=[hbm, vmem, hbm, hbm, hbm],
        out_specs=vmem,
        scratch_shapes=[
            pltpu.VMEM((2, 2, 16, 128, 2 * HP), BF),
            pltpu.VMEM((16, 4, HP, 128), BF),
            pltpu.VMEM((4, T, D), BF),
            pltpu.VMEM((4 * T, D), BF),
            pltpu.VMEM((4 * T, 2 * HP), F32),
            pltpu.VMEM((4 * T, 4 * HP), BF),
            pltpu.VMEM((8, 3, 2, T, 128), BF),
            pltpu.VMEM((3, 8, 2, T, 128), BF),
            pltpu.VMEM((8, T, 256), F32),
            pltpu.VMEM((2, 128, HU), BF),
            dma((4,)),
            dma((4,)),
            dma((4, 16)),
            dma((4,)),
            dma((2,)),
            dma((2, 16)),
            dma((2,)),
            dma((2,)),
            dma(()),
            dma((4,)),
            dma(()),
            dma((3, 8)),
        ],
        compiler_params=pltpu.CompilerParams(
            collective_id=0, has_side_effects=True, vmem_limit_bytes=58 * 2**20
        ),
    )(tokens, norm_gain.reshape(1, D), gate_weight, up_weight, down_weight)


def solution(mesh):
    return jax.shard_map(
        local,
        mesh=mesh,
        in_specs=(P(("fs", "tp"), None), P(), P("fs", "tp"), P("fs", "tp"), P("tp", "fs")),
        out_specs=P(("fs", "tp"), None),
        check_vma=False,
    )
```

time: 262 us -> 108 us (0.41)
  waiting for transfers between devices: 210 us -> 0 us
  Pallas kernels: 0 us -> 102 us
  matrix products: 18 us -> 0 us
  between operations: 13.1 us -> 0.01 us
  starting transfers between devices: 7.12 us -> 0 us
  other arithmetic: 6.96 us -> 0 us
    all_gather x2 -> x0, waiting for transfers between devices: 112 us -> none  [the longest x1 56.7 us: sent_together(): out, at, outs = (lax.all_gather(both, axis, axis=dim, tiled=True), 0, [])]
    pallas_call x0 -> x1, Pallas kernels: none -> 102 us  [local(): pl.pallas_call(kernel, out_shape=jax.ShapeDtypeStruct((T, D), BF), in_spe...]
    reduce_scatter x1 -> x0, waiting for transfers between devices: 98.1 us -> none  [local(): lax.psum_scatter(jnp.dot(hidden, down_local, preferred_element_type=jnp.f...]
    dot_general x3 -> x0, matrix products: 18 us -> none  [the longest x1 8.11 us: local(): jnp.dot(hidden, down_local, preferred_element_type=jnp.float32)]
    all_to_all x1 -> x0, starting transfers between devices: 7.03 us -> none  [from_everyone(): lax.all_to_all(jnp.broadcast_to(x[None], (length, *x.shape)), axis, 0, 0,...]
    convert_element_type x2 -> x0, other arithmetic: 4.11 us -> none  [the longest x1 2.08 us: local(): return mixed.astype(jnp.bfloat16)]
    unnamed x4 -> x5, local copies, waits for them, and re-layouts: 0.64 us -> 4.3 us
  transfers between devices with their start and end apart: 4 -> 0, of which waited for: 3 -> 0; matrix products, arithmetic and copies ran while one was open for 6% -> 0% of each run, Pallas kernels for 0% -> 0%
where the time goes in v1:
time: 108 us; the launch traced here: 106 us
  Pallas kernels  102 us (94%)
  local copies, waits for them, and re-layouts  4.3 us (4%)
    pallas_call x1, Pallas kernels, local(): pl.pallas_call(kernel, out_shape=jax.ShapeDtypeStruct((T, D), BF), in_spe...  102 us
    unnamed x5, local copies, waits for them, and re-layouts  4.3 us

profile of v1, /device:TPU:32, one launch (start us, length us, event | category | flops | bytes accessed | tf_op | source)
XLA Modules:
  0.0 106.3 jit_solution(11337288545675229574)
XLA Ops:
  0.0 0.0 copy-start
  0.0 1.7 %copy.6.gate = bf16[128,352]{1,0:T(8,128)(2,1)} copy(bf16[128,352]{0,1:T(8,128)(2,1)} %param.7) | data formatting | bytes 180224 | tf_op args[2]
  1.7 0.0 copy-done
  1.7 0.8 copy.7.up
  2.4 101.9 %shard_map.55 = bf16[128,2048]{1,0:T(8,128)(2,1)} custom-call(bf16[128,2048]{1,0:T(8,128)(2,1)} %tok.1, f32[1,2048]{1,0:T(1,128)} %bitcast.1, bf16[128,352]{1,0:T(8,128)(2,1)} %copy.6.gate, bf16[128,352]{1,0:T(8,128)(2,1)} %copy.7.up, bf16[352,128]{1,0:T(8,128)(2,1)} %down.1), custom_call_target="tpu_custom_call" | custom-call | tf_op jit(solution)/shard_map/pallas_call | solution.py:265
  104.4 1.9 %copy.9 = bf16[128,2048]{1,0:T(8,128)(2,1)} copy(bf16[128,2048]{1,0:T(8,128)(2,1)} %shard_map.55) | data formatting | bytes 1048576
Async XLA Ops:
  0.0 1.7 %copy-start = (bf16[128,352]{0,1:T(8,128)(2,1)S(1)}, bf16[128,352]{0,1:T(8,128)(2,1)}, u32[]{:S(2)}) copy-start(bf16[128,352]{0,1:T(8,128)(2,1)} %param.8) | copy-start | bytes 270340

commit v2 on v0

v2 whole, which is shorter than its diff:
```python
import jax
import jax.numpy as jnp
from jax import lax
from jax.experimental import pallas as pl
from jax.experimental.pallas import tpu as pltpu
from jax.sharding import PartitionSpec as P

MESH = pl.DeviceIdType.MESH
BF, F32 = jnp.bfloat16, jnp.float32
eps_floor = 0.05

D, T, HU, HP = 2048, 128, 352, 384
GATE_A, UP_A, GATE_B, UP_B, DOWN_A, DOWN_B = range(6)
PAIRS = (((0, 0), (0, 1)), ((1, 0), (-1, 0)), ((1, 1), (0, -1)), ((1, -1), (-1, 1)), ((0, 2), (-1, -1)), ((2, 0), (1, 2)), ((2, 1), (-1, 2)), ((2, -1), (2, 2)))
W, S, C = 0, 1, 2
EVENTS = (
    (C, "own", 0), (C, "own", 1), (C, "own", 4), (S, 0, 0, 0, 0, 1), (S, 0, 0, 0, 0, -1), (S, 0, 0, 0, 1, 1),
    (S, 0, 0, 0, 1, -1), (C, "tokens_out"), (S, 1, 0, 0, 1, 1), (S, 1, 0, 0, 1, -1), (S, 1, 0, 0, 0, 1),
    (S, 1, 0, 0, 0, -1), (S, 4, 0, 0, 0, -1), (W, 0, 0, -1), (W, 0, 0, 1), (W, 0, -1, 0), (W, 0, 1, 0),
    (S, 0, 0, -1, 0, 1), (S, 0, 0, -1, 0, -1), (S, 0, 0, -1, 1, 1), (S, 0, 0, 1, 0, 1), (S, 0, 0, 1, 0, -1),
    (C, "normalize", 0), (W, 1, -1, 0), (W, 1, 1, 0), (W, 1, 0, -1), (W, 1, 0, 1), (S, 1, -1, 0, 0, 1),
    (S, 1, 0, -1, 0, -1), (S, 0, -1, 0, 0, 1), (S, 4, 0, 0, 1, -1), (S, 1, 0, -1, 0, 1), (S, 1, 0, 1, 0, -1),
    (W, 0, -1, -1), (W, 0, -1, 1), (W, 0, 2, 0), (W, 4, 0, 1), (S, 1, 0, -1, 1, 1), (S, 1, 0, 1, 0, 1),
    (S, 0, 2, 0, 1, -1), (W, 0, 1, -1), (W, 0, 1, 1), (W, 1, 0, 2), (W, 1, -1, 1), (C, "plane_b", 0), (C, "own", 2),
    (C, "plane_b", 1), (C, "own", 3), (S, 2, 0, 0, 0, -1), (S, 2, 0, 0, 0, 1), (S, 0, -1, -1, 1, 1),
    (S, 2, 0, 0, 1, -1), (S, 3, 0, 0, 1, -1), (W, 0, 0, 2), (W, 4, 1, 0), (W, 1, -1, -1), (W, 1, 1, 1),
    (S, 1, -1, -1, 1, 1), (S, 0, 2, 0, 1, 1), (S, 3, 0, 0, 0, -1), (W, 1, 2, 0), (S, 1, 2, 0, 1, -1), (W, 1, 1, -1),
    (W, 0, 1, 2), (S, 1, 2, 0, 1, 1), (W, 2, 0, 1), (S, 0, 1, -1, 1, 1), (S, 4, 0, 1, 0, -1), (W, 2, 0, -1),
    (S, 2, 0, 1, 0, -1), (W, 0, 2, -1), (W, 2, 1, 0), (S, 1, 1, -1, 1, 1), (W, 3, 1, 0), (S, 2, 0, 0, 1, 1),
    (W, 1, 2, -1), (S, 2, 0, -1, 0, -1), (W, 0, -1, 2), (W, 3, 0, 1), (S, 3, 0, 1, 0, -1), (S, 0, -1, 2, 0, 1),
    (W, 1, 1, 2), (C, "down_out"), (W, 1, -1, 2), (S, 1, -1, 2, 0, 1), (S, 3, 0, 0, 1, 1), (S, 3, 0, 0, 0, 1),
    (W, 0, 2, 1), (W, 4, 1, 1), (W, 2, 1, 1), (S, 2, 0, 1, 0, 1), (S, 2, 0, -1, 1, 1), (C, "tokens_on"),
    (W, 1, 2, 1), (C, "normalize", 1), (S, 2, 0, -1, 0, 1), (S, 3, 0, 1, 0, 1), (W, 2, -1, 0), (W, 3, 1, 1),
    (W, 2, -1, 1), (C, "tokens_in", 2), (C, "normalize", 2), (S, 2, -1, 0, 0, 1), (W, 0, 2, 2), (W, 1, 2, 2),
    (W, 3, -1, 0), (W, 3, 0, -1), (S, 3, 0, -1, 0, -1), (S, 3, -1, 0, 0, 1), (S, 3, 0, -1, 1, 1), (W, 2, 1, -1),
    (W, 2, 2, 0), (S, 2, 2, 0, 1, -1), (S, 3, 0, -1, 0, 1), (S, 4, 0, 0, 1, 1), (W, 2, -1, -1), (W, 3, 1, -1),
    (S, 3, 1, -1, 1, 1), (S, 2, 1, -1, 1, 1), (W, 2, 0, 2), (W, 3, -1, 1), (S, 2, 2, 0, 1, 1), (W, 3, 2, 0),
    (S, 3, 2, 0, 1, -1), (S, 3, 2, 0, 1, 1), (W, 3, 0, 2), (W, 3, 2, 1), (C, "plane_b", 2), (C, "own", 5),
    (S, 5, 0, 0, 1, -1), (S, 5, 0, 0, 0, -1), (W, 2, 1, 2), (S, 2, -1, -1, 1, 1), (W, 3, -1, -1),
    (S, 3, -1, -1, 1, 1), (W, 4, -1, 0), (C, "tokens_in", 3), (C, "normalize", 3), (S, 5, 0, 0, 0, 1), (W, 2, 2, 1),
    (C, "matmul", True, 0, 0), (W, 3, 1, 2), (S, 4, 0, 0, 0, 1), (W, 3, -1, 2), (S, 3, -1, 2, 0, 1),
    (C, "matmul", True, 0, 1), (W, 2, -1, 2), (S, 2, -1, 2, 0, 1), (S, 4, 0, 1, 0, 1), (W, 5, 1, 0),
    (C, "matmul", True, 0, 2), (W, 5, 0, 1), (S, 5, 0, 1, 0, -1), (S, 5, 0, 1, 0, 1), (C, "gating", True, 0),
    (S, 5, 0, 0, 1, 1), (W, 3, 2, -1), (W, 2, 2, -1), (C, "from_sibling", 0), (C, "matmul", False, 0, 0),
    (W, 5, 0, -1), (W, 3, 2, 2), (S, 5, 0, -1, 0, -1), (S, 4, -1, 0, 0, 1), (S, 5, 0, -1, 0, 1),
    (C, "matmul", False, 0, 1), (C, "matmul", False, 0, 2), (W, 4, 0, -1), (S, 4, 0, -1, 0, -1), (W, 2, 2, 2),
    (C, "gating", False, 0), (S, 4, 0, -1, 1, 1), (S, 5, 0, -1, 1, 1), (W, 4, 1, -1), (C, "matmul", True, 1, 0),
    (W, 5, 1, 1), (S, 4, 1, -1, 1, 1), (S, 4, 0, -1, 0, 1), (C, "matmul", True, 1, 1), (W, 5, -1, 0), (W, 5, 1, -1),
    (C, "matmul", True, 1, 2), (S, 5, -1, 0, 0, 1), (S, 5, 1, -1, 1, 1), (C, "gating", True, 1), (W, 5, -1, 1),
    (W, 4, -1, 1), (W, 5, -1, -1), (W, 4, 0, 2), (S, 5, -1, -1, 1, 1), (C, "from_sibling", 1),
    (C, "matmul", False, 1, 0), (C, "matmul", False, 1, 1), (W, 4, 2, 0), (S, 4, 2, 0, 1, -1), (S, 4, 2, 0, 1, 1),
    (W, 5, 2, 0), (S, 5, 2, 0, 1, -1), (C, "matmul", False, 1, 2), (S, 5, 2, 0, 1, 1), (W, 4, 2, 1), (W, 4, -1, -1),
    (S, 4, -1, -1, 1, 1), (C, "gating", False, 1), (C, "down_pair", 0), (W, 5, 0, 2), (W, 5, 2, 1), (W, 4, 1, 2),
    (W, 5, 1, 2), (C, "down_pair", 1), (W, 4, -1, 2), (S, 4, -1, 2, 0, 1), (W, 5, 2, -1), (W, 4, 2, -1),
    (W, 5, -1, 2), (S, 5, -1, 2, 0, 1), (C, "down_pair", 2), (W, 4, 2, 2), (C, "relay", 0), (W, 5, 2, 2),
    (C, "down_pair", 3), (C, "relay", 1), (C, "down_pair", 4), (C, "relay", 2), (C, "finish", 0),
    (C, "down_pair", 5), (C, "relay", 3), (C, "finish", 1), (C, "down_pair", 6), (C, "relay", 4), (C, "finish", 2),
    (C, "down_pair", 7), (C, "relay", 5), (C, "finish", 3), (C, "relay", 6), (C, "finish", 4), (C, "relay", 7),
    (C, "finish", 5), (C, "finish", 6), (C, "finish", 7),
)


def kernel(tok, gain, gate, up, down, out, wg, wd, x4, nrm, acc, hid, pb, rb, qb, mid, own, ob,
           in_sem, ssem, rsem, dsend, drecv_g, drecv_d, zsend, zrecv, tsend, trecv, psend, precv, osem):
    fs, tp = lax.axis_index("fs"), lax.axis_index("tp")
    y, x, z, c = fs // 4, fs % 4, tp // 2, tp % 2
    d = 1 - 2 * c
    par = (x + y) % 2
    pars = (par, 1 - par, par, 1 - par, 1 - par, par)
    sibling = (fs, z * 2 + 1 - c)

    def zdev(k):
        return (fs, ((z + k * d + 8) % 8) * 2 + c)

    def fpos(t, i, j):
        p = pars[t]
        yy = (y + d * (i * p + j * (1 - p)) + 8) % 4
        xx = (x + d * (i * (1 - p) + j * p) + 8) % 4
        return yy * 4 + xx

    def piece(t, core, f):
        if t < 4:
            return wg.at[core, t // 2, f, t % 2, pl.ds(0, HU), :]
        return wd.at[f, core * 2 + (t - 4), pl.ds(0, HU), :]

    def rcopy(src, dst, s, r, dev):
        return pltpu.make_async_remote_copy(
            src_ref=src, dst_ref=dst, send_sem=s, recv_sem=r, device_id=dev, device_id_type=MESH
        )

    def send(t, i, j, axis, step):
        f = fpos(t, i, j)
        ref = piece(t, c, f)
        to = fpos(t, step, 0) if axis == 0 else fpos(t, 0, step)
        rcopy(ref, ref, ssem.at[t], rsem.at[t, f], (to, tp)).start()

    def across(t, i, j):
        f = fpos(t, i, j)
        ref = piece(t, c, f)
        r = drecv_g.at[t // 2] if t < 4 else drecv_d.at[t - 4, f]
        rcopy(ref, ref, dsend.at[t], r, sibling).start()

    def got(t, i, j):
        f = fpos(t, i, j)
        ref = piece(t, c, f)
        rcopy(ref, ref, ssem.at[t], rsem.at[t, f], sibling).wait_recv()

    def own_ready(t):
        across(t, 0, 0)

    def normalize(slot):
        def rows(i, _):
            at = pl.multiple_of(i * 16, 16)
            v = x4[slot, pl.ds(at, 16), :].astype(F32)
            factor = lax.rsqrt(jnp.sum(v * v, axis=-1, keepdims=True) * (1.0 / D) + eps_floor)
            nrm[pl.ds(pl.multiple_of(slot * T + at, 16), 16), :] = (v * factor * gain[...]).astype(BF)
            return 0

        lax.fori_loop(0, T // 16, rows, 0)

    def matmul(mine, ab, n):
        core = c if mine else 1 - c
        rows = [wg[core, ab, f, h, n * 128 : (n + 1) * 128, :] for h in (0, 1) for f in range(16)]
        w = jnp.concatenate([jnp.concatenate(rows[:16], axis=1), jnp.concatenate(rows[16:], axis=1)], axis=0)
        both = lax.dot_general(nrm[...], w, (((1,), (1,)), ((), ())), preferred_element_type=F32)
        acc[:, n * 256 : (n + 1) * 256] = both

    def gating(mine, ab):
        core = c if mine else 1 - c
        lanes = pl.ds(pl.multiple_of((core * 2 + ab) * HP, 128), HP)

        def rows(i, _):
            at = pl.ds(pl.multiple_of(i * 32, 32), 32)
            v = acc[at, :]
            g = jnp.concatenate([v[:, n * 256 : n * 256 + 128] for n in range(3)], axis=1)
            u = jnp.concatenate([v[:, n * 256 + 128 : n * 256 + 256] for n in range(3)], axis=1)
            hid[at, lanes] = (g / (1.0 + jnp.exp(-g)) * u).astype(BF)
            return 0

        lax.fori_loop(0, 16, rows, 0)

    def from_sibling(ab):
        every = wg.at[1 - c, ab, :, :, pl.ds(0, HU), :]
        rcopy(every, every, dsend.at[ab], drecv_g.at[ab], sibling).wait_recv()

    def pair_fs(p):
        return [fpos(DOWN_A, *o) for o in PAIRS[p]]

    def down_pair(p):
        fa, fb = pair_fs(p)
        for t in (DOWN_A, DOWN_B):
            for f in (fa, fb):
                ref = piece(t, 1 - c, f)
                rcopy(ref, ref, dsend.at[t], drecv_d.at[t - 4, f], sibling).wait_recv()
        w = jnp.concatenate([wd[fa].reshape(4 * HP, 128), wd[fb].reshape(4 * HP, 128)], axis=1)
        part = jnp.dot(hid[...], w, preferred_element_type=F32)
        for s in (3, 2):
            for h in (0, 1):
                pb[s - 1, p, h] = part[s * T : (s + 1) * T, h * 128 : (h + 1) * 128].astype(BF)
        own[p] = part[0:T]
        mid[p] = part[T : 2 * T]
        rcopy(pb.at[2, p], qb.at[p], psend.at[2], precv.at[2, p], zdev(-1)).start()
        rcopy(pb.at[1, p], rb.at[1, p], psend.at[1], precv.at[1, p], zdev(1)).start()

    def relay(p):
        rcopy(qb.at[p], qb.at[p], psend.at[2], precv.at[2, p], sibling).wait_recv()
        for h in (0, 1):
            pb[0, p, h] = (mid[p, :, h * 128 : (h + 1) * 128] + qb[p, h].astype(F32)).astype(BF)
        rcopy(pb.at[0, p], rb.at[0, p], psend.at[0], precv.at[0, p], zdev(-1)).start()

    def finish(p):
        for s in (0, 1):
            rcopy(rb.at[s, p], rb.at[s, p], psend.at[s], precv.at[s, p], sibling).wait_recv()
        for h, f in enumerate(pair_fs(p)):
            v = own[p, :, h * 128 : (h + 1) * 128]
            for s in (0, 1):
                v = v + rb[s, p, h].astype(F32)
            ob[p, h] = v.astype(BF)
            pltpu.make_async_copy(ob.at[p, h], out.at[:, pl.ds(pl.multiple_of(f * 128, 128), 128)], osem).start()

    inputs = [
        pltpu.make_async_copy(gate, piece(GATE_A, c, fs), in_sem.at[0]),
        pltpu.make_async_copy(up, piece(UP_A, c, fs), in_sem.at[1]),
        pltpu.make_async_copy(down, piece(DOWN_A, c, fs), in_sem.at[2]),
        pltpu.make_async_copy(tok, x4.at[0], in_sem.at[3]),
    ]
    for cp in inputs:
        cp.start()
    barrier = pltpu.get_barrier_semaphore()
    partners = [zdev(k) for k in (4, 1, -1)]
    partners += [(fpos(0, *o), tp) for o in ((1, 0), (-1, 0), (0, 1), (0, -1))] + [sibling]
    for dev in partners:
        pl.semaphore_signal(barrier, inc=1, device_id=dev, device_id_type=MESH)
    for f in range(16):
        for b in range(4):
            wd[f, b, HU:HP, :] = jnp.zeros((HP - HU, 128), BF)
            for h in (0, 1):
                wg[b // 2, b % 2, f, h, HU:HP, :] = jnp.zeros((HP - HU, 128), BF)
    for cp in inputs:
        cp.wait()
    pl.semaphore_wait(barrier, len(partners))

    gz = [rcopy(piece(t, c, fs), piece(t + 2, c, fs), zsend.at[t], zrecv.at[t], zdev(4)) for t in (GATE_A, UP_A)]
    dz = rcopy(piece(DOWN_A, c, fs), piece(DOWN_B, c, fs), zsend.at[2], zrecv.at[2], zdev(4))
    t2 = rcopy(x4.at[0], x4.at[2], tsend, trecv.at[2], zdev(-1))
    t1 = rcopy(x4.at[0], x4.at[1], tsend, trecv.at[1], zdev(1))
    t3 = rcopy(x4.at[1], x4.at[3], tsend, trecv.at[3], zdev(1))

    def plane_b(k):
        (gz[0], gz[1], dz)[k].wait_recv()

    def tokens_out():
        for cp in (gz[0], gz[1], t2, t1):
            cp.start()

    def tokens_on():
        t1.wait_recv()
        t3.start()

    def down_out():
        dz.start()

    def tokens_in(k):
        (None, None, t2, t3)[k].wait_recv()

    tasks = {
        "own": own_ready, "plane_b": plane_b, "tokens_out": tokens_out, "tokens_on": tokens_on,
        "down_out": down_out, "tokens_in": tokens_in, "normalize": normalize, "from_sibling": from_sibling,
        "matmul": matmul, "gating": gating, "down_pair": down_pair, "relay": relay, "finish": finish,
    }

    def event(kind, *rest):
        if kind == W:
            got(*rest)
            across(*rest)
        elif kind == S:
            send(*rest)
        else:
            tasks[rest[0]](*rest[1:])

    for e in EVENTS:
        event(*e)

    for t in range(6):
        if t < 4:
            few = wg.at[c, t // 2, pl.ds(0, 15), t % 2, pl.ds(0, HU), :]
            all16 = wg.at[c, t // 2, :, t % 2, pl.ds(0, HU), :]
        else:
            few = wd.at[pl.ds(0, 15), 0, pl.ds(0, HU), :]
            all16 = wd.at[:, 0, pl.ds(0, HU), :]
        rcopy(few, few, ssem.at[t], rsem.at[t, 0], sibling).wait_send()
        rcopy(all16, all16, dsend.at[t], rsem.at[t, 0], sibling).wait_send()
    for cp in (*gz, dz):
        cp.wait_send()
    three = x4.at[pl.ds(0, 3)]
    rcopy(three, three, tsend, trecv.at[1], sibling).wait_send()
    for s in range(3):
        rcopy(pb.at[s], pb.at[s], psend.at[s], precv.at[s, 0], sibling).wait_send()
    pltpu.make_async_copy(x4.at[0], out, osem).wait()


def local(tokens, norm_gain, gate_weight, up_weight, down_weight):
    hbm = pl.BlockSpec(memory_space=pl.ANY)
    vmem = pl.BlockSpec(memory_space=pltpu.VMEM)
    dma = pltpu.SemaphoreType.DMA
    return pl.pallas_call(
        kernel,
        out_shape=jax.ShapeDtypeStruct((T, D), BF),
        in_specs=[hbm, vmem, hbm, hbm, hbm],
        out_specs=hbm,
        scratch_shapes=[
            pltpu.VMEM((2, 2, 16, 2, HP, 128), BF),
            pltpu.VMEM((16, 4, HP, 128), BF),
            pltpu.VMEM((4, T, D), BF),
            pltpu.VMEM((4 * T, D), BF),
            pltpu.VMEM((4 * T, 2 * HP), F32),
            pltpu.VMEM((4 * T, 4 * HP), BF),
            pltpu.VMEM((3, 8, 2, T, 128), BF),
            pltpu.VMEM((2, 8, 2, T, 128), BF),
            pltpu.VMEM((8, 2, T, 128), BF),
            pltpu.VMEM((8, T, 256), F32),
            pltpu.VMEM((8, T, 256), F32),
            pltpu.VMEM((8, 2, T, 128), BF),
            dma((4,)),
            dma((6,)),
            dma((6, 16)),
            dma((6,)),
            dma((2,)),
            dma((2, 16)),
            dma((3,)),
            dma((3,)),
            dma(()),
            dma((4,)),
            dma((3,)),
            dma((3, 8)),
            dma(()),
        ],
        compiler_params=pltpu.CompilerParams(
            collective_id=0, has_side_effects=True, vmem_limit_bytes=58 * 2**20
        ),
    )(tokens, norm_gain.reshape(1, D), gate_weight.T, up_weight.T, down_weight)


def solution(mesh):
    return jax.shard_map(
        local,
        mesh=mesh,
        in_specs=(P(("fs", "tp"), None), P(), P("fs", "tp"), P("fs", "tp"), P("tp", "fs")),
        out_specs=P(("fs", "tp"), None),
        check_vma=False,
    )
```

time: 262 us -> 88.4 us (0.34); the launches traced: 258 us -> 88.2 us
  waiting for transfers between devices: 210 us -> 0 us
  Pallas kernels: 0 us -> 86.3 us
  matrix products: 18 us -> 0 us
  between operations: 13.1 us -> 0.01 us
  starting transfers between devices: 7.12 us -> 0 us
  other arithmetic: 6.96 us -> 0 us
    all_gather x2 -> x0, waiting for transfers between devices: 112 us -> none  [the longest x1 56.7 us: sent_together(): out, at, outs = (lax.all_gather(both, axis, axis=dim, tiled=True), 0, [])]
    reduce_scatter x1 -> x0, waiting for transfers between devices: 98.1 us -> none  [local(): lax.psum_scatter(jnp.dot(hidden, down_local, preferred_element_type=jnp.f...]
    pallas_call x0 -> x1, Pallas kernels: none -> 86.3 us  [local(): pl.pallas_call(kernel, out_shape=jax.ShapeDtypeStruct((T, D), BF), in_spe...]
    dot_general x3 -> x0, matrix products: 18 us -> none  [the longest x1 8.11 us: local(): jnp.dot(hidden, down_local, preferred_element_type=jnp.float32)]
    all_to_all x1 -> x0, starting transfers between devices: 7.03 us -> none  [from_everyone(): lax.all_to_all(jnp.broadcast_to(x[None], (length, *x.shape)), axis, 0, 0,...]
    convert_element_type x2 -> x0, other arithmetic: 4.11 us -> none  [the longest x1 2.08 us: local(): return mixed.astype(jnp.bfloat16)]
  transfers between devices with their start and end apart: 4 -> 0, of which waited for: 3 -> 0; matrix products, arithmetic and copies ran while one was open for 6% -> 0% of each run, Pallas kernels for 0% -> 0%
where the time goes in v2:
time: 88.4 us; the launch traced here: 88.2 us
  Pallas kernels  86.3 us (98%)
  local copies, waits for them, and re-layouts  1.88 us (2%)
    pallas_call x1, Pallas kernels, local(): pl.pallas_call(kernel, out_shape=jax.ShapeDtypeStruct((T, D), BF), in_spe...  86.3 us
    unnamed x1, local copies, waits for them, and re-layouts  1.88 us

profile of v2, /device:TPU:32, one launch (start us, length us, event | category | flops | bytes accessed | tf_op | source)
XLA Modules:
  0.0 88.2 jit_solution(8150799732974869292)
XLA Ops:
  0.0 86.3 %shard_map.55 = bf16[128,2048]{1,0:T(8,128)(2,1)} custom-call(bf16[128,2048]{1,0:T(8,128)(2,1)} %tok.1, f32[1,2048]{1,0:T(1,128)} %bitcast.5, bf16[352,128]{1,0:T(8,128)(2,1)} %bitcast.3, bf16[352,128]{1,0:T(8,128)(2,1)} %bitcast.4, bf16[352,128]{1,0:T(8,128)(2,1)} %down.1), custom_call_target="tpu_custom_call" | custom-call | tf_op jit(solution)/shard_map/pallas_call | solution.py:266
  86.3 1.9 %copy.7 = bf16[128,2048]{1,0:T(8,128)(2,1)} copy(bf16[128,2048]{1,0:T(8,128)(2,1)} %shard_map.55) | data formatting | bytes 1048576

commit v3 on v2

--- a/solution.py
+++ b/solution.py
@@ -11,53 +11,101 @@
 
 D, T, HU, HP = 2048, 128, 352, 384
 GATE_A, UP_A, GATE_B, UP_B, DOWN_A, DOWN_B = range(6)
-PAIRS = (((0, 0), (0, 1)), ((1, 0), (-1, 0)), ((1, 1), (0, -1)), ((1, -1), (-1, 1)), ((0, 2), (-1, -1)), ((2, 0), (1, 2)), ((2, 1), (-1, 2)), ((2, -1), (2, 2)))
+PAIRS = (((0, 0), (-1, 0)), ((1, 0), (0, -1)), ((0, 1), (0, 2)), ((-1, 1), (1, -1)), ((-1, -1), (1, 1)), ((2, -1), (2, 1)), ((2, 0), (-1, 2)), ((1, 2), (2, 2)))
 W, S, C = 0, 1, 2
 EVENTS = (
     (C, "own", 0), (C, "own", 1), (C, "own", 4), (S, 0, 0, 0, 0, 1), (S, 0, 0, 0, 0, -1), (S, 0, 0, 0, 1, 1),
-    (S, 0, 0, 0, 1, -1), (C, "tokens_out"), (S, 1, 0, 0, 1, 1), (S, 1, 0, 0, 1, -1), (S, 1, 0, 0, 0, 1),
-    (S, 1, 0, 0, 0, -1), (S, 4, 0, 0, 0, -1), (W, 0, 0, -1), (W, 0, 0, 1), (W, 0, -1, 0), (W, 0, 1, 0),
+    (S, 0, 0, 0, 1, -1), (S, 1, 0, 0, 1, 1), (S, 1, 0, 0, 1, -1), (S, 1, 0, 0, 0, 1), (S, 1, 0, 0, 0, -1),
+    (C, "tokens_out", 0), (S, 4, 0, 0, 0, -1), (W, 0, 0, -1), (W, 0, 0, 1), (W, 0, -1, 0), (W, 0, 1, 0),
     (S, 0, 0, -1, 0, 1), (S, 0, 0, -1, 0, -1), (S, 0, 0, -1, 1, 1), (S, 0, 0, 1, 0, 1), (S, 0, 0, 1, 0, -1),
-    (C, "normalize", 0), (W, 1, -1, 0), (W, 1, 1, 0), (W, 1, 0, -1), (W, 1, 0, 1), (S, 1, -1, 0, 0, 1),
-    (S, 1, 0, -1, 0, -1), (S, 0, -1, 0, 0, 1), (S, 4, 0, 0, 1, -1), (S, 1, 0, -1, 0, 1), (S, 1, 0, 1, 0, -1),
-    (W, 0, -1, -1), (W, 0, -1, 1), (W, 0, 2, 0), (W, 4, 0, 1), (S, 1, 0, -1, 1, 1), (S, 1, 0, 1, 0, 1),
-    (S, 0, 2, 0, 1, -1), (W, 0, 1, -1), (W, 0, 1, 1), (W, 1, 0, 2), (W, 1, -1, 1), (C, "plane_b", 0), (C, "own", 2),
-    (C, "plane_b", 1), (C, "own", 3), (S, 2, 0, 0, 0, -1), (S, 2, 0, 0, 0, 1), (S, 0, -1, -1, 1, 1),
-    (S, 2, 0, 0, 1, -1), (S, 3, 0, 0, 1, -1), (W, 0, 0, 2), (W, 4, 1, 0), (W, 1, -1, -1), (W, 1, 1, 1),
-    (S, 1, -1, -1, 1, 1), (S, 0, 2, 0, 1, 1), (S, 3, 0, 0, 0, -1), (W, 1, 2, 0), (S, 1, 2, 0, 1, -1), (W, 1, 1, -1),
-    (W, 0, 1, 2), (S, 1, 2, 0, 1, 1), (W, 2, 0, 1), (S, 0, 1, -1, 1, 1), (S, 4, 0, 1, 0, -1), (W, 2, 0, -1),
-    (S, 2, 0, 1, 0, -1), (W, 0, 2, -1), (W, 2, 1, 0), (S, 1, 1, -1, 1, 1), (W, 3, 1, 0), (S, 2, 0, 0, 1, 1),
-    (W, 1, 2, -1), (S, 2, 0, -1, 0, -1), (W, 0, -1, 2), (W, 3, 0, 1), (S, 3, 0, 1, 0, -1), (S, 0, -1, 2, 0, 1),
-    (W, 1, 1, 2), (C, "down_out"), (W, 1, -1, 2), (S, 1, -1, 2, 0, 1), (S, 3, 0, 0, 1, 1), (S, 3, 0, 0, 0, 1),
-    (W, 0, 2, 1), (W, 4, 1, 1), (W, 2, 1, 1), (S, 2, 0, 1, 0, 1), (S, 2, 0, -1, 1, 1), (C, "tokens_on"),
-    (W, 1, 2, 1), (C, "normalize", 1), (S, 2, 0, -1, 0, 1), (S, 3, 0, 1, 0, 1), (W, 2, -1, 0), (W, 3, 1, 1),
-    (W, 2, -1, 1), (C, "tokens_in", 2), (C, "normalize", 2), (S, 2, -1, 0, 0, 1), (W, 0, 2, 2), (W, 1, 2, 2),
-    (W, 3, -1, 0), (W, 3, 0, -1), (S, 3, 0, -1, 0, -1), (S, 3, -1, 0, 0, 1), (S, 3, 0, -1, 1, 1), (W, 2, 1, -1),
-    (W, 2, 2, 0), (S, 2, 2, 0, 1, -1), (S, 3, 0, -1, 0, 1), (S, 4, 0, 0, 1, 1), (W, 2, -1, -1), (W, 3, 1, -1),
-    (S, 3, 1, -1, 1, 1), (S, 2, 1, -1, 1, 1), (W, 2, 0, 2), (W, 3, -1, 1), (S, 2, 2, 0, 1, 1), (W, 3, 2, 0),
-    (S, 3, 2, 0, 1, -1), (S, 3, 2, 0, 1, 1), (W, 3, 0, 2), (W, 3, 2, 1), (C, "plane_b", 2), (C, "own", 5),
-    (S, 5, 0, 0, 1, -1), (S, 5, 0, 0, 0, -1), (W, 2, 1, 2), (S, 2, -1, -1, 1, 1), (W, 3, -1, -1),
-    (S, 3, -1, -1, 1, 1), (W, 4, -1, 0), (C, "tokens_in", 3), (C, "normalize", 3), (S, 5, 0, 0, 0, 1), (W, 2, 2, 1),
-    (C, "matmul", True, 0, 0), (W, 3, 1, 2), (S, 4, 0, 0, 0, 1), (W, 3, -1, 2), (S, 3, -1, 2, 0, 1),
-    (C, "matmul", True, 0, 1), (W, 2, -1, 2), (S, 2, -1, 2, 0, 1), (S, 4, 0, 1, 0, 1), (W, 5, 1, 0),
-    (C, "matmul", True, 0, 2), (W, 5, 0, 1), (S, 5, 0, 1, 0, -1), (S, 5, 0, 1, 0, 1), (C, "gating", True, 0),
-    (S, 5, 0, 0, 1, 1), (W, 3, 2, -1), (W, 2, 2, -1), (C, "from_sibling", 0), (C, "matmul", False, 0, 0),
-    (W, 5, 0, -1), (W, 3, 2, 2), (S, 5, 0, -1, 0, -1), (S, 4, -1, 0, 0, 1), (S, 5, 0, -1, 0, 1),
-    (C, "matmul", False, 0, 1), (C, "matmul", False, 0, 2), (W, 4, 0, -1), (S, 4, 0, -1, 0, -1), (W, 2, 2, 2),
-    (C, "gating", False, 0), (S, 4, 0, -1, 1, 1), (S, 5, 0, -1, 1, 1), (W, 4, 1, -1), (C, "matmul", True, 1, 0),
-    (W, 5, 1, 1), (S, 4, 1, -1, 1, 1), (S, 4, 0, -1, 0, 1), (C, "matmul", True, 1, 1), (W, 5, -1, 0), (W, 5, 1, -1),
-    (C, "matmul", True, 1, 2), (S, 5, -1, 0, 0, 1), (S, 5, 1, -1, 1, 1), (C, "gating", True, 1), (W, 5, -1, 1),
-    (W, 4, -1, 1), (W, 5, -1, -1), (W, 4, 0, 2), (S, 5, -1, -1, 1, 1), (C, "from_sibling", 1),
-    (C, "matmul", False, 1, 0), (C, "matmul", False, 1, 1), (W, 4, 2, 0), (S, 4, 2, 0, 1, -1), (S, 4, 2, 0, 1, 1),
-    (W, 5, 2, 0), (S, 5, 2, 0, 1, -1), (C, "matmul", False, 1, 2), (S, 5, 2, 0, 1, 1), (W, 4, 2, 1), (W, 4, -1, -1),
-    (S, 4, -1, -1, 1, 1), (C, "gating", False, 1), (C, "down_pair", 0), (W, 5, 0, 2), (W, 5, 2, 1), (W, 4, 1, 2),
-    (W, 5, 1, 2), (C, "down_pair", 1), (W, 4, -1, 2), (S, 4, -1, 2, 0, 1), (W, 5, 2, -1), (W, 4, 2, -1),
-    (W, 5, -1, 2), (S, 5, -1, 2, 0, 1), (C, "down_pair", 2), (W, 4, 2, 2), (C, "relay", 0), (W, 5, 2, 2),
-    (C, "down_pair", 3), (C, "relay", 1), (C, "down_pair", 4), (C, "relay", 2), (C, "finish", 0),
-    (C, "down_pair", 5), (C, "relay", 3), (C, "finish", 1), (C, "down_pair", 6), (C, "relay", 4), (C, "finish", 2),
-    (C, "down_pair", 7), (C, "relay", 5), (C, "finish", 3), (C, "relay", 6), (C, "finish", 4), (C, "relay", 7),
-    (C, "finish", 5), (C, "finish", 6), (C, "finish", 7),
+    (S, 0, -1, 0, 0, 1), (C, "normalize", 0), (S, 4, 0, 0, 1, -1), (W, 1, -1, 0), (W, 1, 1, 0), (W, 1, 0, -1),
+    (W, 1, 0, 1), (S, 1, -1, 0, 0, 1), (S, 1, 0, -1, 0, -1), (S, 1, 0, -1, 0, 1), (S, 1, 0, 1, 0, -1),
+    (S, 1, 0, -1, 1, 1), (S, 1, 0, 1, 0, 1), (W, 0, -1, -1), (W, 0, -1, 1), (W, 0, 2, 0), (W, 4, 0, 1),
+    (S, 0, 2, 0, 1, -1), (S, 0, -1, -1, 1, 1), (S, 0, 2, 0, 1, 1), (W, 0, 1, -1), (W, 0, 1, 1), (W, 1, 0, 2),
+    (W, 1, -1, 1), (S, 0, 1, -1, 1, 1), (C, "plane_b", 0), (C, "own", 2), (C, "plane_b", 1), (C, "own", 3),
+    (S, 2, 0, 0, 0, -1), (S, 2, 0, 0, 0, 1), (S, 2, 0, 0, 1, -1), (S, 3, 0, 0, 1, -1), (S, 3, 0, 0, 0, -1),
+    (S, 2, 0, 0, 1, 1), (S, 3, 0, 0, 1, 1), (S, 3, 0, 0, 0, 1), (C, "tokens_out", 1), (W, 0, 0, 2), (W, 4, 1, 0),
+    (W, 1, -1, -1), (W, 1, 1, 1), (S, 1, -1, -1, 1, 1), (W, 1, 2, 0), (S, 1, 2, 0, 1, -1), (S, 1, 2, 0, 1, 1),
+    (S, 4, 0, 1, 0, -1), (W, 1, 1, -1), (W, 0, 1, 2), (S, 1, 1, -1, 1, 1), (W, 2, 0, 1), (S, 2, 0, 1, 0, -1),
+    (S, 2, 0, 1, 0, 1), (W, 2, 0, -1), (S, 2, 0, -1, 0, -1), (S, 2, 0, -1, 1, 1), (S, 2, 0, -1, 0, 1),
+    (W, 0, 2, -1), (W, 2, 1, 0), (C, "tokens_on"), (W, 3, 1, 0), (W, 1, 2, -1), (C, "normalize", 1), (W, 0, -1, 2),
+    (W, 3, 0, 1), (S, 3, 0, 1, 0, -1), (S, 0, -1, 2, 0, 1), (S, 3, 0, 1, 0, 1), (W, 1, 1, 2), (W, 1, -1, 2),
+    (S, 1, -1, 2, 0, 1), (W, 0, 2, 1), (W, 4, 1, 1), (W, 2, 1, 1), (W, 1, 2, 1), (W, 2, -1, 0), (W, 3, 1, 1),
+    (S, 2, -1, 0, 0, 1), (W, 2, -1, 1), (W, 0, 2, 2), (W, 1, 2, 2), (C, "down_out"), (W, 3, -1, 0), (W, 3, 0, -1),
+    (S, 3, 0, -1, 0, -1), (S, 3, -1, 0, 0, 1), (S, 3, 0, -1, 1, 1), (S, 3, 0, -1, 0, 1), (S, 4, 0, 0, 1, 1),
+    (W, 2, 1, -1), (W, 2, 2, 0), (S, 2, 2, 0, 1, -1), (S, 2, 1, -1, 1, 1), (S, 2, 2, 0, 1, 1), (W, 2, -1, -1),
+    (S, 2, -1, -1, 1, 1), (W, 3, 1, -1), (S, 3, 1, -1, 1, 1), (W, 2, 0, 2), (W, 3, -1, 1), (W, 3, 2, 0),
+    (S, 3, 2, 0, 1, -1), (S, 3, 2, 0, 1, 1), (W, 3, 0, 2), (S, 4, 0, 0, 0, 1), (C, "tokens_in", 2),
+    (C, "normalize", 2), (W, 3, 2, 1), (C, "tokens_in", 3), (C, "normalize", 3), (W, 2, 1, 2), (W, 3, -1, -1),
+    (S, 3, -1, -1, 1, 1), (W, 4, -1, 0), (S, 4, 0, 1, 0, 1),
 )
+GATE_EVENTS = {
+    1: (
+        (W, 2, 2, 1),
+    ),
+    2: (
+        (S, 4, -1, 0, 0, 1), (W, 3, 1, 2), (W, 3, -1, 2), (W, 2, -1, 2), (S, 2, -1, 2, 0, 1), (S, 3, -1, 2, 0, 1),
+    ),
+    4: (
+        (W, 3, 2, -1), (W, 2, 2, -1), (C, "from_sibling", 0),
+    ),
+    5: (
+        (W, 4, 0, -1), (S, 4, 0, -1, 1, 1), (S, 4, 0, -1, 0, -1), (S, 4, 0, -1, 0, 1),
+    ),
+    6: (
+        (C, "plane_b", 2), (C, "own", 5), (S, 5, 0, 0, 0, -1), (S, 5, 0, 0, 0, 1), (S, 5, 0, 0, 1, -1),
+    ),
+    7: (
+        (W, 2, 2, 2), (W, 3, 2, 2), (S, 5, 0, 0, 1, 1),
+    ),
+    8: (
+        (W, 4, 1, -1), (S, 4, 1, -1, 1, 1),
+    ),
+    10: (
+        (W, 4, 2, 0), (S, 4, 2, 0, 1, -1), (S, 4, 2, 0, 1, 1),
+    ),
+    11: (
+        (W, 4, -1, 1), (W, 4, 0, 2), (W, 5, 0, 1), (S, 5, 0, 1, 0, -1), (S, 5, 0, 1, 0, 1),
+    ),
+    12: (
+        (W, 5, 0, -1), (S, 5, 0, -1, 1, 1), (C, "from_sibling", 1),
+    ),
+    13: (
+        (S, 5, 0, -1, 0, -1), (S, 5, 0, -1, 0, 1),
+    ),
+    14: (
+        (W, 5, 1, 0), (W, 4, -1, -1), (W, 4, 2, 1),
+    ),
+    15: (
+        (W, 5, -1, 0),
+    ),
+}
+DOWN_EVENTS = {
+    0: (
+        (S, 4, -1, -1, 1, 1), (W, 4, 1, 2),
+    ),
+    1: (
+        (W, 5, 2, 0), (S, 5, 2, 0, 1, 1), (S, 5, 2, 0, 1, -1), (W, 4, -1, 2), (S, 4, -1, 2, 0, 1),
+        (S, 5, -1, 0, 0, 1), (W, 5, 1, 1),
+    ),
+    2: (
+        (W, 5, 1, -1), (S, 5, 1, -1, 1, 1), (W, 5, -1, 1), (W, 5, -1, -1), (W, 5, -1, 2), (W, 5, 1, 2),
+        (S, 5, -1, 2, 0, 1), (S, 5, -1, -1, 1, 1),
+    ),
+    3: (
+        (W, 4, 2, -1), (W, 4, 2, 2), (W, 5, 0, 2), (W, 5, 2, 1),
+    ),
+    4: (
+        (W, 5, 2, 2), (W, 5, 2, -1),
+    ),
+    9: (
+        (C, "drain", 0), (C, "drain", 1), (C, "drain", 2), (C, "drain", 3), (C, "drain", 6),
+    ),
+    10: (
+        (C, "drain", 4), (C, "drain", 5),
+    ),
+}
+LAG = 2
 
 
 def kernel(tok, gain, gate, up, down, out, wg, wd, x4, nrm, acc, hid, pb, rb, qb, mid, own, ob,
@@ -118,15 +166,25 @@
 
         lax.fori_loop(0, T // 16, rows, 0)
 
-    def matmul(mine, ab, n):
-        core = c if mine else 1 - c
-        rows = [wg[core, ab, f, h, n * 128 : (n + 1) * 128, :] for h in (0, 1) for f in range(16)]
-        w = jnp.concatenate([jnp.concatenate(rows[:16], axis=1), jnp.concatenate(rows[16:], axis=1)], axis=0)
-        both = lax.dot_general(nrm[...], w, (((1,), (1,)), ((), ())), preferred_element_type=F32)
-        acc[:, n * 256 : (n + 1) * 256] = both
-
-    def gating(mine, ab):
-        core = c if mine else 1 - c
+    def block_of(b):
+        return (1 - c if b % 2 else c), b // 2
+
+    def matmul(b):
+        core, ab = block_of(b)
+
+        def columns(n, _):
+            events_at({m: GATE_EVENTS[4 * b + m] for m in (1, 2) if 4 * b + m in GATE_EVENTS}, n)
+            at = pl.ds(pl.multiple_of(n * 128, 128), 128)
+            rows = [wg[core, ab, f, h, at, :] for h in (0, 1) for f in range(16)]
+            w = jnp.concatenate([jnp.concatenate(rows[:16], axis=1), jnp.concatenate(rows[16:], axis=1)], axis=0)
+            both = lax.dot_general(nrm[...], w, (((1,), (1,)), ((), ())), preferred_element_type=F32)
+            acc[:, pl.ds(pl.multiple_of(n * 256, 256), 256)] = both
+            return 0
+
+        lax.fori_loop(0, 3, columns, 0)
+
+    def gating(b):
+        core, ab = block_of(b)
         lanes = pl.ds(pl.multiple_of((core * 2 + ab) * HP, 128), HP)
 
         def rows(i, _):
@@ -144,7 +202,14 @@
         rcopy(every, every, dsend.at[ab], drecv_g.at[ab], sibling).wait_recv()
 
     def pair_fs(p):
-        return [fpos(DOWN_A, *o) for o in PAIRS[p]]
+        picked = []
+        for h in (0, 1):
+            i, j = PAIRS[0][h]
+            for k in range(1, 8):
+                i = jnp.where(p == k, PAIRS[k][h][0], i)
+                j = jnp.where(p == k, PAIRS[k][h][1], j)
+            picked.append(fpos(DOWN_A, i, j))
+        return picked
 
     def down_pair(p):
         fa, fb = pair_fs(p)
@@ -209,8 +274,8 @@
     def plane_b(k):
         (gz[0], gz[1], dz)[k].wait_recv()
 
-    def tokens_out():
-        for cp in (gz[0], gz[1], t2, t1):
+    def tokens_out(k):
+        for cp in ((gz[0], gz[1], t1), (t2,))[k]:
             cp.start()
 
     def tokens_on():
@@ -223,10 +288,25 @@
     def tokens_in(k):
         (None, None, t2, t3)[k].wait_recv()
 
+    def drain(t):
+        if t < 4:
+            few = wg.at[c, t // 2, pl.ds(0, 15), t % 2, pl.ds(0, HU), :]
+            all16 = wg.at[c, t // 2, :, t % 2, pl.ds(0, HU), :]
+        elif t < 6:
+            few = wd.at[pl.ds(0, 15), 0, pl.ds(0, HU), :]
+            all16 = wd.at[:, 0, pl.ds(0, HU), :]
+        else:
+            for cp in (*gz, dz):
+                cp.wait_send()
+            three = x4.at[pl.ds(0, 3)]
+            rcopy(three, three, tsend, trecv.at[1], sibling).wait_send()
+            return
+        rcopy(few, few, ssem.at[t], rsem.at[t, 0], sibling).wait_send()
+        rcopy(all16, all16, dsend.at[t], rsem.at[t, 0], sibling).wait_send()
+
     tasks = {
         "own": own_ready, "plane_b": plane_b, "tokens_out": tokens_out, "tokens_on": tokens_on,
-        "down_out": down_out, "tokens_in": tokens_in, "normalize": normalize, "from_sibling": from_sibling,
-        "matmul": matmul, "gating": gating, "down_pair": down_pair, "relay": relay, "finish": finish,
+        "down_out": down_out, "tokens_in": tokens_in, "normalize": normalize, "from_sibling": from_sibling, "drain": drain,
     }
 
     def event(kind, *rest):
@@ -238,22 +318,44 @@
         else:
             tasks[rest[0]](*rest[1:])
 
+    def events_at(table, k):
+        for at, some in table.items():
+
+            @pl.when(k == at)
+            def _():
+                for e in some:
+                    event(*e)
+
     for e in EVENTS:
         event(*e)
 
-    for t in range(6):
-        if t < 4:
-            few = wg.at[c, t // 2, pl.ds(0, 15), t % 2, pl.ds(0, HU), :]
-            all16 = wg.at[c, t // 2, :, t % 2, pl.ds(0, HU), :]
-        else:
-            few = wd.at[pl.ds(0, 15), 0, pl.ds(0, HU), :]
-            all16 = wd.at[:, 0, pl.ds(0, HU), :]
-        rcopy(few, few, ssem.at[t], rsem.at[t, 0], sibling).wait_send()
-        rcopy(all16, all16, dsend.at[t], rsem.at[t, 0], sibling).wait_send()
-    for cp in (*gz, dz):
-        cp.wait_send()
-    three = x4.at[pl.ds(0, 3)]
-    rcopy(three, three, tsend, trecv.at[1], sibling).wait_send()
+    for b in range(4):
+        for e in GATE_EVENTS.get(4 * b, ()):
+            event(*e)
+        matmul(b)
+        for e in GATE_EVENTS.get(4 * b + 3, ()):
+            event(*e)
+        gating(b)
+
+    def down_step(k, _):
+        events_at(DOWN_EVENTS, k)
+
+        @pl.when(k < 8)
+        def _():
+            down_pair(k)
+
+        @pl.when((k >= LAG) & (k < 8 + LAG))
+        def _():
+            relay(k - LAG)
+
+        @pl.when(k >= 2 * LAG)
+        def _():
+            finish(k - 2 * LAG)
+
+        return 0
+
+    lax.fori_loop(0, 8 + 2 * LAG, down_step, 0)
+
     for s in range(3):
         rcopy(pb.at[s], pb.at[s], psend.at[s], precv.at[s, 0], sibling).wait_send()
     pltpu.make_async_copy(x4.at[0], out, osem).wait()

time: 88.4 us -> 85.1 us (0.963)
  Pallas kernels: 86.3 us -> 82.8 us
    pallas_call x1, Pallas kernels: 86.3 us -> 82.8 us  [local(): pl.pallas_call(kernel, out_shape=jax.ShapeDtypeStruct((T, D), BF), in_spe...]
where the time goes in v3:
time: 85.1 us; the launch traced here: 84.7 us
  Pallas kernels  82.8 us (97%)
  local copies, waits for them, and re-layouts  1.88 us (2%)
    pallas_call x1, Pallas kernels, local(): pl.pallas_call(kernel, out_shape=jax.ShapeDtypeStruct((T, D), BF), in_spe...  82.8 us
    unnamed x1, local copies, waits for them, and re-layouts  1.88 us

profile of v3, /device:TPU:32, one launch (start us, length us, event | category | flops | bytes accessed | tf_op | source)
XLA Modules:
  0.0 84.7 jit_solution(15696879328916033734)
XLA Ops:
  0.0 82.8 %shard_map.55 = bf16[128,2048]{1,0:T(8,128)(2,1)} custom-call(bf16[128,2048]{1,0:T(8,128)(2,1)} %tok.1, f32[1,2048]{1,0:T(1,128)} %bitcast.5, bf16[352,128]{1,0:T(8,128)(2,1)} %bitcast.3, bf16[352,128]{1,0:T(8,128)(2,1)} %bitcast.4, bf16[352,128]{1,0:T(8,128)(2,1)} %down.1), custom_call_target="tpu_custom_call" | custom-call | tf_op jit(solution)/shard_map/pallas_call | solution.py:368
  82.8 1.9 %copy.7 = bf16[128,2048]{1,0:T(8,128)(2,1)} copy(bf16[128,2048]{1,0:T(8,128)(2,1)} %shard_map.55) | data formatting | bytes 1048576

commit v4 on v3

--- a/solution.py
+++ b/solution.py
@@ -16,35 +16,35 @@
 EVENTS = (
     (C, "own", 0), (C, "own", 1), (C, "own", 4), (S, 0, 0, 0, 0, 1), (S, 0, 0, 0, 0, -1), (S, 0, 0, 0, 1, 1),
     (S, 0, 0, 0, 1, -1), (S, 1, 0, 0, 1, 1), (S, 1, 0, 0, 1, -1), (S, 1, 0, 0, 0, 1), (S, 1, 0, 0, 0, -1),
-    (C, "tokens_out", 0), (S, 4, 0, 0, 0, -1), (W, 0, 0, -1), (W, 0, 0, 1), (W, 0, -1, 0), (W, 0, 1, 0),
-    (S, 0, 0, -1, 0, 1), (S, 0, 0, -1, 0, -1), (S, 0, 0, -1, 1, 1), (S, 0, 0, 1, 0, 1), (S, 0, 0, 1, 0, -1),
-    (S, 0, -1, 0, 0, 1), (C, "normalize", 0), (S, 4, 0, 0, 1, -1), (W, 1, -1, 0), (W, 1, 1, 0), (W, 1, 0, -1),
+    (S, 4, 0, 0, 0, -1), (C, "tokens_out", 0), (S, 4, 0, 0, 1, -1), (W, 0, 0, -1), (W, 0, 0, 1), (W, 0, -1, 0),
+    (W, 0, 1, 0), (S, 0, 0, -1, 0, 1), (S, 0, 0, -1, 0, -1), (S, 0, 0, -1, 1, 1), (S, 0, 0, 1, 0, 1),
+    (S, 0, 0, 1, 0, -1), (S, 0, -1, 0, 0, 1), (C, "normalize", 0), (W, 1, -1, 0), (W, 1, 1, 0), (W, 1, 0, -1),
     (W, 1, 0, 1), (S, 1, -1, 0, 0, 1), (S, 1, 0, -1, 0, -1), (S, 1, 0, -1, 0, 1), (S, 1, 0, 1, 0, -1),
     (S, 1, 0, -1, 1, 1), (S, 1, 0, 1, 0, 1), (W, 0, -1, -1), (W, 0, -1, 1), (W, 0, 2, 0), (W, 4, 0, 1),
     (S, 0, 2, 0, 1, -1), (S, 0, -1, -1, 1, 1), (S, 0, 2, 0, 1, 1), (W, 0, 1, -1), (W, 0, 1, 1), (W, 1, 0, 2),
-    (W, 1, -1, 1), (S, 0, 1, -1, 1, 1), (C, "plane_b", 0), (C, "own", 2), (C, "plane_b", 1), (C, "own", 3),
-    (S, 2, 0, 0, 0, -1), (S, 2, 0, 0, 0, 1), (S, 2, 0, 0, 1, -1), (S, 3, 0, 0, 1, -1), (S, 3, 0, 0, 0, -1),
-    (S, 2, 0, 0, 1, 1), (S, 3, 0, 0, 1, 1), (S, 3, 0, 0, 0, 1), (C, "tokens_out", 1), (W, 0, 0, 2), (W, 4, 1, 0),
-    (W, 1, -1, -1), (W, 1, 1, 1), (S, 1, -1, -1, 1, 1), (W, 1, 2, 0), (S, 1, 2, 0, 1, -1), (S, 1, 2, 0, 1, 1),
-    (S, 4, 0, 1, 0, -1), (W, 1, 1, -1), (W, 0, 1, 2), (S, 1, 1, -1, 1, 1), (W, 2, 0, 1), (S, 2, 0, 1, 0, -1),
-    (S, 2, 0, 1, 0, 1), (W, 2, 0, -1), (S, 2, 0, -1, 0, -1), (S, 2, 0, -1, 1, 1), (S, 2, 0, -1, 0, 1),
-    (W, 0, 2, -1), (W, 2, 1, 0), (C, "tokens_on"), (W, 3, 1, 0), (W, 1, 2, -1), (C, "normalize", 1), (W, 0, -1, 2),
-    (W, 3, 0, 1), (S, 3, 0, 1, 0, -1), (S, 0, -1, 2, 0, 1), (S, 3, 0, 1, 0, 1), (W, 1, 1, 2), (W, 1, -1, 2),
-    (S, 1, -1, 2, 0, 1), (W, 0, 2, 1), (W, 4, 1, 1), (W, 2, 1, 1), (W, 1, 2, 1), (W, 2, -1, 0), (W, 3, 1, 1),
-    (S, 2, -1, 0, 0, 1), (W, 2, -1, 1), (W, 0, 2, 2), (W, 1, 2, 2), (C, "down_out"), (W, 3, -1, 0), (W, 3, 0, -1),
-    (S, 3, 0, -1, 0, -1), (S, 3, -1, 0, 0, 1), (S, 3, 0, -1, 1, 1), (S, 3, 0, -1, 0, 1), (S, 4, 0, 0, 1, 1),
-    (W, 2, 1, -1), (W, 2, 2, 0), (S, 2, 2, 0, 1, -1), (S, 2, 1, -1, 1, 1), (S, 2, 2, 0, 1, 1), (W, 2, -1, -1),
-    (S, 2, -1, -1, 1, 1), (W, 3, 1, -1), (S, 3, 1, -1, 1, 1), (W, 2, 0, 2), (W, 3, -1, 1), (W, 3, 2, 0),
-    (S, 3, 2, 0, 1, -1), (S, 3, 2, 0, 1, 1), (W, 3, 0, 2), (S, 4, 0, 0, 0, 1), (C, "tokens_in", 2),
-    (C, "normalize", 2), (W, 3, 2, 1), (C, "tokens_in", 3), (C, "normalize", 3), (W, 2, 1, 2), (W, 3, -1, -1),
-    (S, 3, -1, -1, 1, 1), (W, 4, -1, 0), (S, 4, 0, 1, 0, 1),
+    (W, 1, -1, 1), (S, 0, 1, -1, 1, 1), (S, 4, 0, 1, 0, -1), (C, "plane_b", 0), (C, "own", 2), (C, "plane_b", 1),
+    (C, "own", 3), (S, 2, 0, 0, 0, -1), (S, 2, 0, 0, 0, 1), (S, 2, 0, 0, 1, -1), (S, 3, 0, 0, 1, -1),
+    (S, 3, 0, 0, 0, -1), (S, 2, 0, 0, 1, 1), (S, 3, 0, 0, 1, 1), (S, 3, 0, 0, 0, 1), (C, "tokens_out", 1),
+    (W, 0, 0, 2), (W, 4, 1, 0), (W, 1, -1, -1), (W, 1, 1, 1), (S, 1, -1, -1, 1, 1), (W, 1, 2, 0),
+    (S, 1, 2, 0, 1, -1), (S, 1, 2, 0, 1, 1), (W, 1, 1, -1), (W, 0, 1, 2), (S, 1, 1, -1, 1, 1), (W, 2, 0, 1),
+    (S, 2, 0, 1, 0, -1), (S, 2, 0, 1, 0, 1), (W, 2, 0, -1), (S, 2, 0, -1, 0, -1), (S, 2, 0, -1, 1, 1),
+    (S, 2, 0, -1, 0, 1), (W, 0, 2, -1), (W, 2, 1, 0), (C, "tokens_on"), (W, 3, 1, 0), (W, 1, 2, -1),
+    (C, "normalize", 1), (W, 0, -1, 2), (W, 3, 0, 1), (S, 3, 0, 1, 0, -1), (S, 0, -1, 2, 0, 1), (S, 3, 0, 1, 0, 1),
+    (W, 1, 1, 2), (W, 1, -1, 2), (S, 1, -1, 2, 0, 1), (W, 0, 2, 1), (W, 4, 1, 1), (W, 2, 1, 1), (W, 1, 2, 1),
+    (S, 4, 0, 0, 1, 1), (W, 2, -1, 0), (W, 3, 1, 1), (S, 2, -1, 0, 0, 1), (W, 2, -1, 1), (W, 0, 2, 2), (W, 1, 2, 2),
+    (C, "down_out"), (W, 3, -1, 0), (W, 3, 0, -1), (S, 3, 0, -1, 0, -1), (S, 3, -1, 0, 0, 1), (S, 3, 0, -1, 1, 1),
+    (S, 3, 0, -1, 0, 1), (W, 2, 1, -1), (W, 2, 2, 0), (S, 2, 2, 0, 1, -1), (S, 2, 1, -1, 1, 1), (S, 2, 2, 0, 1, 1),
+    (S, 4, 0, 0, 0, 1), (W, 2, -1, -1), (S, 2, -1, -1, 1, 1), (W, 3, 1, -1), (S, 3, 1, -1, 1, 1), (W, 2, 0, 2),
+    (S, 4, 0, 1, 0, 1), (W, 3, -1, 1), (W, 3, 2, 0), (S, 3, 2, 0, 1, -1), (S, 3, 2, 0, 1, 1), (W, 3, 0, 2),
+    (C, "tokens_in", 2), (C, "normalize", 2), (W, 3, 2, 1), (C, "tokens_in", 3), (C, "normalize", 3), (W, 2, 1, 2),
+    (W, 3, -1, -1), (S, 3, -1, -1, 1, 1), (W, 4, -1, 0), (S, 4, -1, 0, 0, 1),
 )
 GATE_EVENTS = {
     1: (
         (W, 2, 2, 1),
     ),
     2: (
-        (S, 4, -1, 0, 0, 1), (W, 3, 1, 2), (W, 3, -1, 2), (W, 2, -1, 2), (S, 2, -1, 2, 0, 1), (S, 3, -1, 2, 0, 1),
+        (W, 3, 1, 2), (W, 3, -1, 2), (W, 2, -1, 2), (S, 2, -1, 2, 0, 1), (S, 3, -1, 2, 0, 1),
     ),
     4: (
         (W, 3, 2, -1), (W, 2, 2, -1), (C, "from_sibling", 0),
@@ -54,9 +54,10 @@
     ),
     6: (
         (C, "plane_b", 2), (C, "own", 5), (S, 5, 0, 0, 0, -1), (S, 5, 0, 0, 0, 1), (S, 5, 0, 0, 1, -1),
+        (S, 5, 0, 0, 1, 1),
     ),
     7: (
-        (W, 2, 2, 2), (W, 3, 2, 2), (S, 5, 0, 0, 1, 1),
+        (W, 2, 2, 2), (W, 3, 2, 2),
     ),
     8: (
         (W, 4, 1, -1), (S, 4, 1, -1, 1, 1),
@@ -68,25 +69,21 @@
         (W, 4, -1, 1), (W, 4, 0, 2), (W, 5, 0, 1), (S, 5, 0, 1, 0, -1), (S, 5, 0, 1, 0, 1),
     ),
     12: (
-        (W, 5, 0, -1), (S, 5, 0, -1, 1, 1), (C, "from_sibling", 1),
-    ),
-    13: (
-        (S, 5, 0, -1, 0, -1), (S, 5, 0, -1, 0, 1),
+        (W, 5, 0, -1), (S, 5, 0, -1, 1, 1), (S, 5, 0, -1, 0, -1), (S, 5, 0, -1, 0, 1), (C, "from_sibling", 1),
     ),
     14: (
-        (W, 5, 1, 0), (W, 4, -1, -1), (W, 4, 2, 1),
+        (W, 5, 1, 0), (W, 4, -1, -1), (S, 4, -1, -1, 1, 1), (W, 4, 2, 1),
     ),
     15: (
-        (W, 5, -1, 0),
+        (W, 5, -1, 0), (S, 5, -1, 0, 0, 1),
     ),
 }
 DOWN_EVENTS = {
     0: (
-        (S, 4, -1, -1, 1, 1), (W, 4, 1, 2),
+        (W, 4, 1, 2),
     ),
     1: (
-        (W, 5, 2, 0), (S, 5, 2, 0, 1, 1), (S, 5, 2, 0, 1, -1), (W, 4, -1, 2), (S, 4, -1, 2, 0, 1),
-        (S, 5, -1, 0, 0, 1), (W, 5, 1, 1),
+        (W, 5, 2, 0), (S, 5, 2, 0, 1, 1), (S, 5, 2, 0, 1, -1), (W, 4, -1, 2), (S, 4, -1, 2, 0, 1), (W, 5, 1, 1),
     ),
     2: (
         (W, 5, 1, -1), (S, 5, 1, -1, 1, 1), (W, 5, -1, 1), (W, 5, -1, -1), (W, 5, -1, 2), (W, 5, 1, 2),
@@ -105,10 +102,10 @@
         (C, "drain", 4), (C, "drain", 5),
     ),
 }
-LAG = 2
-
-
-def kernel(tok, gain, gate, up, down, out, wg, wd, x4, nrm, acc, hid, pb, rb, qb, mid, own, ob,
+LAG = 3
+
+
+def kernel(tok, gain_in, gate, up, down, out, gain, wg, wd, x4, nrm, acc, hid, pb, rb, qb, mid, own, ob,
            in_sem, ssem, rsem, dsend, drecv_g, drecv_d, zsend, zrecv, tsend, trecv, psend, precv, osem):
     fs, tp = lax.axis_index("fs"), lax.axis_index("tp")
     y, x, z, c = fs // 4, fs % 4, tp // 2, tp % 2
@@ -248,14 +245,15 @@
         pltpu.make_async_copy(up, piece(UP_A, c, fs), in_sem.at[1]),
         pltpu.make_async_copy(down, piece(DOWN_A, c, fs), in_sem.at[2]),
         pltpu.make_async_copy(tok, x4.at[0], in_sem.at[3]),
+        pltpu.make_async_copy(gain_in, gain, in_sem.at[4]),
     ]
-    for cp in inputs:
-        cp.start()
     barrier = pltpu.get_barrier_semaphore()
     partners = [zdev(k) for k in (4, 1, -1)]
     partners += [(fpos(0, *o), tp) for o in ((1, 0), (-1, 0), (0, 1), (0, -1))] + [sibling]
     for dev in partners:
         pl.semaphore_signal(barrier, inc=1, device_id=dev, device_id_type=MESH)
+    for cp in inputs:
+        cp.start()
     for f in range(16):
         for b in range(4):
             wd[f, b, HU:HP, :] = jnp.zeros((HP - HU, 128), BF)
@@ -363,14 +361,14 @@
 
 def local(tokens, norm_gain, gate_weight, up_weight, down_weight):
     hbm = pl.BlockSpec(memory_space=pl.ANY)
-    vmem = pl.BlockSpec(memory_space=pltpu.VMEM)
     dma = pltpu.SemaphoreType.DMA
     return pl.pallas_call(
         kernel,
         out_shape=jax.ShapeDtypeStruct((T, D), BF),
-        in_specs=[hbm, vmem, hbm, hbm, hbm],
+        in_specs=[hbm] * 5,
         out_specs=hbm,
         scratch_shapes=[
+            pltpu.VMEM((1, D), F32),
             pltpu.VMEM((2, 2, 16, 2, HP, 128), BF),
             pltpu.VMEM((16, 4, HP, 128), BF),
             pltpu.VMEM((4, T, D), BF),
@@ -383,7 +381,7 @@
             pltpu.VMEM((8, T, 256), F32),
             pltpu.VMEM((8, T, 256), F32),
             pltpu.VMEM((8, 2, T, 128), BF),
-            dma((4,)),
+            dma((5,)),
             dma((6,)),
             dma((6, 16)),
             dma((6,)),

time: 85.1 us -> 83.2 us (0.978)
  Pallas kernels: 82.8 us -> 81.2 us
    pallas_call x1, Pallas kernels: 82.8 us -> 81.2 us  [local(): pl.pallas_call(kernel, out_shape=jax.ShapeDtypeStruct((T, D), BF), in_spe...]
where the time goes in v4:
time: 83.2 us; the launch traced here: 83 us
  Pallas kernels  81.2 us (98%)
  local copies, waits for them, and re-layouts  1.88 us (2%)
    pallas_call x1, Pallas kernels, local(): pl.pallas_call(kernel, out_shape=jax.ShapeDtypeStruct((T, D), BF), in_spe...  81.2 us
    unnamed x1, local copies, waits for them, and re-layouts  1.88 us

profile of v4, /device:TPU:32, one launch (start us, length us, event | category | flops | bytes accessed | tf_op | source)
XLA Modules:
  0.0 83.0 jit_solution(10185603390205101989)
XLA Ops:
  0.0 81.2 %shard_map.55 = bf16[128,2048]{1,0:T(8,128)(2,1)} custom-call(bf16[128,2048]{1,0:T(8,128)(2,1)} %tok.1, f32[1,2048]{1,0:T(1,128)} %bitcast.5, bf16[352,128]{1,0:T(8,128)(2,1)} %bitcast.3, bf16[352,128]{1,0:T(8,128)(2,1)} %bitcast.4, bf16[352,128]{1,0:T(8,128)(2,1)} %down.1), custom_call_target="tpu_custom_call" | custom-call | tf_op jit(solution)/shard_map/pallas_call | solution.py:365
  81.2 1.9 %copy.7 = bf16[128,2048]{1,0:T(8,128)(2,1)} copy(bf16[128,2048]{1,0:T(8,128)(2,1)} %shard_map.55) | data formatting | bytes 1048576

commit v5 on v4

--- a/solution.py
+++ b/solution.py
@@ -102,7 +102,7 @@
         (C, "drain", 4), (C, "drain", 5),
     ),
 }
-LAG = 3
+LAG = 4
 
 
 def kernel(tok, gain_in, gate, up, down, out, gain, wg, wd, x4, nrm, acc, hid, pb, rb, qb, mid, own, ob,

time: 83.2 us -> 83.4 us (level)
  no operation moved by 1% of the time
where the time goes in v5:
time: 83.4 us; the launch traced here: 83.3 us
  Pallas kernels  81.4 us (98%)
  local copies, waits for them, and re-layouts  1.88 us (2%)
    pallas_call x1, Pallas kernels, local(): pl.pallas_call(kernel, out_shape=jax.ShapeDtypeStruct((T, D), BF), in_spe...  81.4 us
    unnamed x1, local copies, waits for them, and re-layouts  1.88 us

profile of v5, /device:TPU:32, one launch (start us, length us, event | category | flops | bytes accessed | tf_op | source)
XLA Modules:
  0.0 83.3 jit_solution(15524397980745813357)
XLA Ops:
  0.0 81.4 %shard_map.55 = bf16[128,2048]{1,0:T(8,128)(2,1)} custom-call(bf16[128,2048]{1,0:T(8,128)(2,1)} %tok.1, f32[1,2048]{1,0:T(1,128)} %bitcast.5, bf16[352,128]{1,0:T(8,128)(2,1)} %bitcast.3, bf16[352,128]{1,0:T(8,128)(2,1)} %bitcast.4, bf16[352,128]{1,0:T(8,128)(2,1)} %down.1), custom_call_target="tpu_custom_call" | custom-call | tf_op jit(solution)/shard_map/pallas_call | solution.py:365
  81.4 1.9 %copy.7 = bf16[128,2048]{1,0:T(8,128)(2,1)} copy(bf16[128,2048]{1,0:T(8,128)(2,1)} %shard_map.55) | data formatting | bytes 1048576
